TPU v7x, 256 devices: a 8x8x2 block of a 8x8x16 slice. The times are simulated.
256 devices in a mesh: grp: 2 (over z), ep: 16 (over y, core), tp: 8 (over x).
Axes of the slice: x: 8, y: 8, z: 2, core: 2. Of those that a mesh axis runs over, the one named last changes fastest.
The devices are a block of a 8x8x16 slice.
Arguments:
- tokens: bfloat16 [8192, 4096], P(('grp', 'ep')), parts along dimension 0, may hold values from -6 to 6
- expert_ids: int32 [8192, 2], P(('grp', 'ep')), parts along dimension 0, may hold values from 0 to 15, as said below
- gates: float32 [8192, 2], P(('grp', 'ep')), parts along dimension 0, may hold values from 0.1 to 1
- w_gate: bfloat16 [16, 4096, 2048], P('ep', None, 'tp'), may hold values from -0.09375 to 0.09375
- w_up: bfloat16 [16, 4096, 2048], P('ep', None, 'tp'), may hold values from -0.09375 to 0.09375
- w_down: bfloat16 [16, 2048, 4096], P('ep', 'tp'), may hold values from -0.79549513 to 0.79549513, as said below
- norm_gain: float32 [4096], P('tp'), may hold values from 0.1 to 1.9
- norm_bias: float32 [4096], P('tp'), may hold values from -1.5 to 1.5
Outputs:
- normed: bfloat16 [8192, 4096], P(('grp', 'ep'), 'tp'), parts along dimension 0
There are 2 independent parts, one for each index of `grp`. A program takes and returns all parts, laid end to end along the dimension named above; an argument that names none is the same for every part. Nothing has to cross between parts.
Inputs may be any that keep to these rules, and one draw needn't show every extreme that they name: `expert_ids`: each row names 2 different experts, both in the same group of 4 consecutive expert numbers. Within one aligned block of 256 rows no expert is named more than 64 times, and in every draw some expert is named exactly 64 times in every block. `w_down`: down projection weights.
All inputs are finite; a program needn't handle non-finite values.
Results may differ from a plain program's by a relative error of at most 0.014.
Values may be sent and summed in bfloat16 or wider, within the bound.
No kernel may reach another device: no remote copies, remote signals or barrier semaphores. Data moves between devices by JAX's collectives and lax.ppermute only.
A program may use at most 128 MiB of HBM per device.

v0:
```python
import jax
import jax.numpy as jnp
from jax import lax
from jax.sharding import PartitionSpec as P

D = 4096
TOPK = 2
EXPERTS = 16
CAP = 64
norm_eps = 1e-05


def copy_for_each(value, axis):
    peers = lax.axis_size(axis)
    return lax.all_to_all(
        jnp.broadcast_to(value[None], (peers, *value.shape)), axis, 0, 0, tiled=True
    )


def of_everyone(value, axis):
    everything = copy_for_each(value, axis)
    return jnp.sum(everything, axis=0)


def together(arrays, axis):
    ends = [0]
    for a in arrays:
        ends.append(ends[-1] + a.size)
    subtotal = of_everyone(jnp.concatenate([a.ravel() for a in arrays]), axis)
    return tuple((subtotal[b:e].reshape(a.shape) for a, b, e in zip(arrays, ends, ends[1:])))


def route_slots(expert_ids):
    flat_ids = expert_ids.reshape(-1)
    onehot = (flat_ids[:, None] == jnp.arange(EXPERTS, dtype=jnp.int32)[None, :]).astype(jnp.int32)
    position = jnp.sum((jnp.cumsum(onehot, axis=0) - 1) * onehot, axis=1)
    target = flat_ids * CAP + position
    token_of = jnp.arange(flat_ids.shape[0], dtype=jnp.int32) // TOPK
    source = jnp.zeros((EXPERTS * CAP,), jnp.int32).at[target].set(token_of)
    filled = jnp.zeros((EXPERTS * CAP,), jnp.bool_).at[target].set(True)
    return (target, source, filled)


def on_device(tokens, expert_ids, gates, w_gate, w_up, w_down, norm_gain, norm_bias):
    tok_rows, width = tokens.shape
    piece_width = norm_gain.shape[0]
    target, source, filled = route_slots(expert_ids)
    offset = lax.axis_index("tp") * piece_width
    own_columns = lax.dynamic_slice_in_dim(tokens, offset, piece_width, 1)
    outgoing = jnp.where(filled[:, None], own_columns[source], jnp.zeros((), jnp.bfloat16)).reshape(
        EXPERTS, CAP, piece_width
    )
    arrived = lax.all_to_all(outgoing, "ep", split_axis=0, concat_axis=1, tiled=True)
    segment = lax.all_gather(arrived, "tp", axis=2, tiled=True)
    gate_more = jnp.einsum("erd,edf->erf", segment, w_gate, preferred_element_type=jnp.float32)
    up_more = jnp.einsum("erd,edf->erf", segment, w_up, preferred_element_type=jnp.float32)
    hidden = (jax.nn.silu(gate_more) * up_more).astype(jnp.bfloat16)
    partial_value = jnp.einsum("erf,efd->erd", hidden, w_down, preferred_element_type=jnp.float32)
    summed = lax.psum_scatter(
        partial_value.astype(jnp.bfloat16), "tp", scatter_dimension=2, tiled=True
    )
    returned = lax.all_to_all(summed, "ep", split_axis=1, concat_axis=0, tiled=True)
    picked = returned.reshape(EXPERTS * CAP, piece_width)[target].reshape(
        tok_rows, TOPK, piece_width
    )
    combined = jnp.sum(picked.astype(jnp.float32) * gates[:, :, None], axis=1)
    stats = together((jnp.sum(combined, axis=1), jnp.sum(combined * combined, axis=1)), "tp")
    row_mean = stats[0] / D
    row_var = stats[1] / D - row_mean * row_mean
    normed = (combined - row_mean[:, None]) * lax.rsqrt(
        row_var[:, None] + norm_eps
    ) * norm_gain + norm_bias
    return normed.astype(jnp.bfloat16)


def solution(mesh):
    return jax.shard_map(
        on_device,
        mesh=mesh,
        in_specs=(
            P(("grp", "ep"), None),
            P(("grp", "ep"), None),
            P(("grp", "ep"), None),
            P("ep", None, "tp"),
            P("ep", None, "tp"),
            P("ep", "tp", None),
            P("tp"),
            P("tp"),
        ),
        out_specs=P(("grp", "ep"), "tp"),
        check_vma=False,
    )
```

profile of v0, /device:TPU:513, one launch (start us, length us, event | category | flops | bytes accessed | tf_op | source)
XLA Modules:
  0.0 358.6 jit_solution(16169199813096574413)
XLA Ops:
  6.5 0.0 copy-start
  6.6 0.0 all-gather.2.cloned.1.call-start
  6.6 1.0 copy.38
  7.5 0.1 eq.29
  7.7 0.1 eq.25
  7.8 0.7 broadcast_multiply_fusion
  8.5 1.2 reduce-window.6
  9.7 0.2 slice_reduce_fusion
  9.9 0.1 copy.37
  10.1 0.1 mul.70
  10.2 0.1 fusion.18
  10.3 2.4 scatter_custom_fusion.1
  12.8 2.4 scatter_custom_fusion
  15.3 0.1 broadcast_in_dim.24
  15.3 1.0 constant_dynamic-slice_fusion
  16.3 4.0 %gather_fusion = bf16[1024,512]{1,0:T(8,128)(2,1)S(1)} fusion(bf16[256,512]{1,0:T(8,128)(2,1)S(1)} %constant_dynamic-slice_fusion, s32[1024]{0:T(1024)S(1)} %fusion.20), kind=kCustom, calls=%fused_computation | custom fusion | bytes 2101248 | tf_op jit(solution)/shard_map/gather | solution.py:50
  20.3 0.2 broadcast_select_fusion
  20.5 52.0 %all_to_all.27 = bf16[16,64,512]{2,1,0:T(8,128)(2,1)} all-to-all(bf16[16,64,512]{2,1,0:T(8,128)(2,1)S(1)} %broadcast_select_fusion), channel_id=1, replica_groups=mesh['grp'=2,'ep'=16,'tp'=8] {'ep'}, dimensions={0} | all-to-all | bytes 2097152 | tf_op jit(solution)/shard_map/all_to_all | solution.py:53
  72.5 0.1 all-gather.2.cloned.1.call-update
  72.5 0.2 reduce-scatter.2.cloned.1.call-start
  72.8 92.8 %all-gather.2.cloned.1.call-done = bf16[1,1024,4096]{2,1,0:T(8,128)(2,1)} async-done(((bf16[1,1024,512]{2,1,0:T(8,128)(2,1)}), bf16[1,1024,4096]{2,1,0:T(8,128)(2,1)}) %all-gather.2.cloned.1.call-update) | async-done | bytes 8388624 | tf_op jit(solution)/shard_map/all_gather | solution.py:54
  165.6 0.0 copy-start.5
  165.6 0.0 copy-start.6
  165.6 6.5 %fusion.2 = f32[1024,256]{1,0:T(8,128)S(1)} fusion(bf16[1,1024,4096]{2,1,0:T(8,128)(2,1)} %all-gather.2.cloned.1.call-done, bf16[1,4096,256]{2,1,0:T(8,128)(2,1)} %param.11), kind=kOutput, calls=%fused_computation.6 | convolution fusion | flops 2147483648 | bytes 11534336 | tf_op jit(solution)/shard_map/erd,edf->erf/dot_general | solution.py:55
  172.1 0.0 copy-done.5
  172.1 0.5 copy-done.6
  172.6 2.4 fusion.12
  174.9 0.0 copy-done
  174.9 5.6 %convert_bitcast_fusion = bf16[1,1024,4096]{2,1,0:T(8,128)(2,1)} fusion(bf16[1024,256]{1,0:T(8,128)(2,1)S(1)} %fusion.12, bf16[1,256,4096]{2,1,0:T(8,128)(2,1)S(1)} %copy-done), kind=kOutput, calls=%fused_computation.8 | convolution fusion | flops 2151677952 | bytes 11010048 | tf_op jit(solution)/shard_map/erf,efd->erd/dot_general | solution.py:58
  180.5 0.1 reduce-scatter.2.cloned.1.call-update
  180.6 95.3 %reduce-scatter.2.cloned.1.call-done = bf16[1,1024,512]{2,1,0:T(8,128)(2,1)} async-done(((bf16[1,1024,4096]{2,1,0:T(8,128)(2,1)}), bf16[1,1024,512]{2,1,0:T(8,128)(2,1)}) %reduce-scatter.2.cloned.1.call-update) | async-done | bytes 1048592 | tf_op jit(solution)/shard_map/reduce_scatter | solution.py:59
  275.8 4.2 %copy.54 = bf16[1,1024,512]{2,0,1:T(2,128)(2,1)} copy(bf16[1,1024,512]{2,1,0:T(8,128)(2,1)} %reduce-scatter.2.cloned.1.call-done) | data formatting | bytes 2097152 | tf_op jit(solution)/shard_map/reduce_scatter | solution.py:59
  280.0 0.5 broadcast.121
  280.5 8.3 %reduce.6 = bf16[1024,512]{1,0:T(8,128)(2,1)S(1)} reduce(bf16[1024,1,512]{2,1,0:T(2,128)(2,1)} %bitcast.53, bf16[]{:T(256)} %broadcast.121), dimensions={1}, to_apply=%bitcast.50.reduce_sub_computation | reduce | bytes 2097154
  288.8 0.0 copy-start.2
  288.8 1.6 reshape.155
  290.4 7.7 %all-to-all-start.1 = ((bf16[16,2,16384]{2,1,0:T(2,128)(2,1)}), bf16[16,2,16384]{2,1,0:T(2,128)(2,1)S(1)}, u32[]{:S(2)}, u32[]{:S(2)}) async-start(bf16[16,2,16384]{2,1,0:T(2,128)(2,1)} %reshape.155), calls=%async_computation.2 | async-start | bytes 2097152 | tf_op jit(solution)/shard_map/all_to_all | solution.py:62
  298.1 0.0 copy-done.2
  298.1 0.1 copy.42
  298.3 0.1 mul.77
  298.4 27.7 %all-to-all-done.1 = bf16[16,2,16384]{2,1,0:T(2,128)(2,1)S(1)} async-done(((bf16[16,2,16384]{2,1,0:T(2,128)(2,1)}), bf16[16,2,16384]{2,1,0:T(2,128)(2,1)S(1)}, u32[]{:S(2)}, u32[]{:S(2)}) %all-to-all-start.1) | async-done | bytes 1048608 | tf_op jit(solution)/shard_map/all_to_all | solution.py:62
  326.1 3.5 reshape.156
  329.6 1.9 copy.53
  331.4 2.6 gather_fusion.1
  334.1 0.0 copy-start.1
  334.1 0.0 copy-start.3
  334.1 0.0 copy-start.4
  334.1 2.8 reshape.116
  336.8 2.6 multiply_reduce_fusion.1
  339.4 0.1 multiply_reduce_fusion.2
  339.6 0.0 copy-done.1
  339.6 0.3 multiply_reduce_fusion
  339.8 0.1 reduce_sum.58
  340.0 0.1 reduce_sum.59
  340.1 10.7 %all_to_all.28 = f32[8,1,512]{2,1,0:T(1,128)S(1)} all-to-all(f32[8,1,512]{2,1,0:T(1,128)S(1)} %broadcast_in_dim.45), channel_id=1, replica_groups=mesh['grp'=2,'ep'=16,'tp'=8] {'tp'}, dimensions={0} | all-to-all | bytes 32768 | tf_op jit(solution)/shard_map/all_to_all | solution.py:15
  350.8 0.0 copy-done.3
  350.9 0.0 copy-done.4
  350.9 0.9 add_convert_fusion
  (12 shorter events, 0.1 us)
Async XLA Ops:
  6.5 168.4 %copy-start = (bf16[1,256,4096]{2,1,0:T(8,128)(2,1)S(1)}, bf16[1,256,4096]{2,1,0:T(8,128)(2,1)}, u32[]{:S(2)}) copy-start(bf16[1,256,4096]{2,1,0:T(8,128)(2,1)} %param.13) | copy-start | bytes 6291460
  6.6 159.0 %all-gather.2.cloned.1.call-start = ((), (), s32[]{:S(2)}) async-start(), calls=%async_computation.4 | async-start | bytes 9437184 | tf_op jit(solution)/shard_map/all_gather | solution.py:54
  72.5 203.3 %reduce-scatter.2.cloned.1.call-start = ((), (), s32[]{:S(2)}) async-start(), calls=%async_computation.5 | async-start | bytes 9437184 | tf_op jit(solution)/shard_map/reduce_scatter | solution.py:59
  165.6 6.5 %copy-start.5 = (bf16[1,1024,4096]{2,1,0:T(8,128)(2,1)S(1)}, bf16[1,1024,4096]{2,1,0:T(8,128)(2,1)}, u32[]{:S(2)}) copy-start(bf16[1,1024,4096]{2,1,0:T(8,128)(2,1)} %all-gather.2.cloned.1.call-done) | copy-start | bytes 25165828
  165.6 7.0 %copy-start.6 = (bf16[1,4096,256]{2,1,0:T(8,128)(2,1)S(1)}, bf16[1,4096,256]{2,1,0:T(8,128)(2,1)}, u32[]{:S(2)}) copy-start(bf16[1,4096,256]{2,1,0:T(8,128)(2,1)} %param.12) | copy-start | bytes 6291460
  288.8 9.3 %copy-start.2 = (f32[256,2]{0,1:T(2,128)S(1)}, f32[256,2]{0,1:T(2,128)}, u32[]{:S(2)}) copy-start(f32[256,2]{0,1:T(2,128)} %param.10) | copy-start | bytes 6148
  290.4 35.7 %all-to-all-start.1 = ((bf16[16,2,16384]{2,1,0:T(2,128)(2,1)}), bf16[16,2,16384]{2,1,0:T(2,128)(2,1)S(1)}, u32[]{:S(2)}, u32[]{:S(2)}) async-start(bf16[16,2,16384]{2,1,0:T(2,128)(2,1)} %reshape.155), calls=%async_computation.2 | async-start | bytes 2097152 | tf_op jit(solution)/shard_map/all_to_all | solution.py:62
  334.1 5.5 %copy-start.1 = (bf16[512,512]{1,0:T(8,128)(2,1)S(1)}, bf16[512,512]{1,0:T(8,128)(2,1)}, u32[]{:S(2)}) copy-start(bf16[512,512]{1,0:T(8,128)(2,1)} %gather_fusion.1) | copy-start | bytes 1572868
  334.1 16.8 %copy-start.3 = (f32[512]{0:T(512)S(1)}, f32[512]{0:T(512)}, u32[]{:S(2)}) copy-start(f32[512]{0:T(512)} %param.15) | copy-start | bytes 6148
  334.1 16.8 %copy-start.4 = (f32[512]{0:T(512)S(1)}, f32[512]{0:T(512)}, u32[]{:S(2)}) copy-start(f32[512]{0:T(512)} %param.14) | copy-start | bytes 6148
Sparse Core Ops, SparseCore 0:
  72.7 92.8 all-gather.1
  180.7 95.0 reduce-scatter.1
where the time goes:
time: 359 us
  waiting for transfers between devices  216 us (60%)
  blocking collectives  62.7 us (17%)
  local copies, waits for them, and re-layouts  29.6 us (8%)
  other arithmetic  14.4 us (4%)
  matrix products  14.4 us (4%)
  between operations  13.7 us (4%)
  starting transfers between devices  7.98 us (2%)
    reduce_scatter x1, waiting for transfers between devices, on_device(): lax.psum_scatter(partial_value.astype(jnp.bfloat16), 'tp', scatter_dimens...  95.3 us
    all_gather x1, waiting for transfers between devices, on_device(): segment = lax.all_gather(arrived, 'tp', axis=2, tiled=True)  92.8 us
    all_to_all x1, blocking collectives, on_device(): lax.all_to_all(outgoing, 'ep', split_axis=0, concat_axis=1, tiled=True)  52 us
    all_to_all x1, waiting for transfers between devices, on_device(): lax.all_to_all(summed, 'ep', split_axis=1, concat_axis=0, tiled=True)  27.7 us
    all_to_all x1, blocking collectives, copy_for_each(): lax.all_to_all(jnp.broadcast_to(value[None], (peers, *value.shape)), axis...  10.7 us
    unnamed x20, local copies, waits for them, and re-layouts  9.03 us
    unnamed x1, other arithmetic  8.25 us
    all_to_all x1, starting transfers between devices, on_device(): lax.all_to_all(summed, 'ep', split_axis=1, concat_axis=0, tiled=True)  7.73 us
  transfers between devices with their start and end apart: 3, of which 3 were waited for; matrix products, arithmetic and copies ran while one was open for 0% of the time, Pallas kernels for 0%

commit v1 on v0

--- a/solution.py
+++ b/solution.py
@@ -51,7 +51,9 @@
         EXPERTS, CAP, piece_width
     )
     arrived = lax.all_to_all(outgoing, "ep", split_axis=0, concat_axis=1, tiled=True)
-    segment = lax.all_gather(arrived, "tp", axis=2, tiled=True)
+    segment = jnp.concatenate(
+        lax.all_to_all(jnp.stack([arrived] * lax.axis_size("tp")), "tp", 0, 0), axis=2
+    )
     gate_more = jnp.einsum("erd,edf->erf", segment, w_gate, preferred_element_type=jnp.float32)
     up_more = jnp.einsum("erd,edf->erf", segment, w_up, preferred_element_type=jnp.float32)
     hidden = (jax.nn.silu(gate_more) * up_more).astype(jnp.bfloat16)

time: 359 us -> 451 us (1.26)
  blocking collectives: 62.7 us -> 251 us
  waiting for transfers between devices: 216 us -> 121 us
    all_to_all x0 -> x1, blocking collectives: none -> 189 us  [on_device(): lax.all_to_all(jnp.stack([arrived] * lax.axis_size('tp')), 'tp', 0, 0)]
    all_gather x1 -> x0, waiting for transfers between devices: 92.8 us -> none  [on_device(): segment = lax.all_gather(arrived, 'tp', axis=2, tiled=True)]
  transfers between devices with their start and end apart: 3 -> 2, of which waited for: 3 -> 2; matrix products, arithmetic and copies ran while one was open for 0% -> 0% of each run, Pallas kernels for 0% -> 0%
where the time goes in v1:
time: 451 us; the launch traced here: 450 us
  blocking collectives  251 us (56%)
  waiting for transfers between devices  121 us (27%)
  local copies, waits for them, and re-layouts  31.7 us (7%)
  other arithmetic  14.4 us (3%)
  between operations  13.7 us (3%)
  matrix products  10.4 us (2%)
  starting transfers between devices  7.73 us (2%)
    all_to_all x1, blocking collectives, on_device(): lax.all_to_all(jnp.stack([arrived] * lax.axis_size('tp')), 'tp', 0, 0)  189 us
    reduce_scatter x1, waiting for transfers between devices, on_device(): lax.psum_scatter(partial_value.astype(jnp.bfloat16), 'tp', scatter_dimens...  93.5 us
    all_to_all x1, blocking collectives, on_device(): lax.all_to_all(outgoing, 'ep', split_axis=0, concat_axis=1, tiled=True)  52 us
    all_to_all x1, waiting for transfers between devices, on_device(): lax.all_to_all(summed, 'ep', split_axis=1, concat_axis=0, tiled=True)  27.7 us
    all_to_all x1, blocking collectives, copy_for_each(): lax.all_to_all(jnp.broadcast_to(value[None], (peers, *value.shape)), axis...  10.7 us
  transfers between devices with their start and end apart: 2, of which 2 were waited for; matrix products, arithmetic and copies ran while one was open for 0% of the time, Pallas kernels for 0%

profile of v1, /device:TPU:513, one launch (start us, length us, event | category | flops | bytes accessed | tf_op | source)
XLA Modules:
  0.0 450.4 jit_solution(9942144403006005476)
XLA Ops:
  6.5 0.0 copy-start
  6.6 0.0 reduce-scatter.2.cloned.1.call-start
  6.6 1.0 copy.45
  7.5 0.1 eq.29
  7.7 0.1 eq.25
  7.8 0.7 broadcast_multiply_fusion
  8.5 1.2 reduce-window.6
  9.7 0.2 slice_reduce_fusion
  9.9 0.1 copy.44
  10.1 0.1 mul.70
  10.2 0.1 fusion.12
  10.3 2.4 scatter_custom_fusion.1
  12.8 2.4 scatter_custom_fusion
  15.3 0.1 broadcast_in_dim.24
  15.3 1.0 constant_dynamic-slice_fusion
  16.3 4.0 gather_fusion
  20.3 0.2 broadcast_select_fusion
  20.5 52.0 %all_to_all.29 = bf16[16,64,512]{2,1,0:T(8,128)(2,1)} all-to-all(bf16[16,64,512]{2,1,0:T(8,128)(2,1)S(1)} %broadcast_select_fusion), channel_id=1, replica_groups=mesh['grp'=2,'ep'=16,'tp'=8] {'ep'}, dimensions={0} | all-to-all | bytes 2097152 | tf_op jit(solution)/shard_map/all_to_all | solution.py:53
  72.5 1.5 copy.48
  74.0 1.1 stack.5
  75.0 0.0 copy-start.2
  75.0 188.6 %all_to_all.30 = bf16[8,1,1024,512]{2,3,1,0:T(8,128)(2,1)S(1)} all-to-all(bf16[8,1,1024,512]{2,3,1,0:T(8,128)(2,1)S(1)} %stack.5), channel_id=1, replica_groups=mesh['grp'=2,'ep'=16,'tp'=8] {'tp'}, dimensions={0} | all-to-all | bytes 16777216 | tf_op jit(solution)/shard_map/all_to_all | solution.py:55
  263.6 0.0 copy-done.2
  263.6 0.0 copy-start.6
  263.6 2.4 fusion.3
  266.0 0.0 copy-done.6
  266.0 2.4 fusion.8
  268.4 0.0 copy-done
  268.4 5.6 %convert_bitcast_fusion = bf16[1,1024,4096]{2,1,0:T(8,128)(2,1)} fusion(bf16[1024,256]{1,0:T(8,128)(2,1)S(1)} %fusion.8, bf16[1,256,4096]{2,1,0:T(8,128)(2,1)S(1)} %copy-done), kind=kOutput, calls=%fused_computation.4 | convolution fusion | flops 2151677952 | bytes 11010048 | tf_op jit(solution)/shard_map/erf,efd->erd/dot_general | solution.py:60
  274.0 0.1 reduce-scatter.2.cloned.1.call-update
  274.1 93.5 %reduce-scatter.2.cloned.1.call-done = bf16[1,1024,512]{2,1,0:T(8,128)(2,1)} async-done(((bf16[1,1024,4096]{2,1,0:T(8,128)(2,1)}), bf16[1,1024,512]{2,1,0:T(8,128)(2,1)}) %reduce-scatter.2.cloned.1.call-update) | async-done | bytes 1048592 | tf_op jit(solution)/shard_map/reduce_scatter | solution.py:61
  367.6 4.2 copy.63
  371.8 0.5 broadcast.123
  372.3 8.3 %reduce.6 = bf16[1024,512]{1,0:T(8,128)(2,1)S(1)} reduce(bf16[1024,1,512]{2,1,0:T(2,128)(2,1)} %bitcast.53, bf16[]{:T(256)} %broadcast.123), dimensions={1}, to_apply=%bitcast.48.reduce_sub_computation | reduce | bytes 2097154
  380.6 0.0 copy-start.3
  380.6 1.6 reshape.167
  382.2 7.7 %all-to-all-start.2 = ((bf16[16,2,16384]{2,1,0:T(2,128)(2,1)}), bf16[16,2,16384]{2,1,0:T(2,128)(2,1)S(1)}, u32[]{:S(2)}, u32[]{:S(2)}) async-start(bf16[16,2,16384]{2,1,0:T(2,128)(2,1)} %reshape.167), calls=%async_computation.3 | async-start | bytes 2097152 | tf_op jit(solution)/shard_map/all_to_all | solution.py:64
  389.9 0.0 copy-done.3
  389.9 0.1 copy.51
  390.1 0.1 mul.77
  390.2 27.7 %all-to-all-done.2 = bf16[16,2,16384]{2,1,0:T(2,128)(2,1)S(1)} async-done(((bf16[16,2,16384]{2,1,0:T(2,128)(2,1)}), bf16[16,2,16384]{2,1,0:T(2,128)(2,1)S(1)}, u32[]{:S(2)}, u32[]{:S(2)}) %all-to-all-start.2) | async-done | bytes 1048608 | tf_op jit(solution)/shard_map/all_to_all | solution.py:64
  417.9 3.5 reshape.168
  421.4 1.9 copy.62
  423.2 2.6 gather_fusion.1
  425.9 0.0 copy-start.1
  425.9 0.0 copy-start.4
  425.9 0.0 copy-start.5
  425.9 2.8 reshape.128
  428.6 2.6 multiply_reduce_fusion.1
  431.2 0.1 multiply_reduce_fusion.2
  431.3 0.0 copy-done.1
  431.4 0.3 multiply_reduce_fusion
  431.6 0.1 reduce_sum.58
  431.8 0.1 reduce_sum.59
  431.9 10.7 %all_to_all.31 = f32[8,1,512]{2,1,0:T(1,128)S(1)} all-to-all(f32[8,1,512]{2,1,0:T(1,128)S(1)} %broadcast_in_dim.45), channel_id=1, replica_groups=mesh['grp'=2,'ep'=16,'tp'=8] {'tp'}, dimensions={0} | all-to-all | bytes 32768 | tf_op jit(solution)/shard_map/all_to_all | solution.py:15
  442.6 0.0 copy-done.4
  442.6 0.0 copy-done.5
  442.7 0.9 add_convert_fusion
  (12 shorter events, 0.1 us)
Async XLA Ops:
  6.5 261.9 %copy-start = (bf16[1,256,4096]{2,1,0:T(8,128)(2,1)S(1)}, bf16[1,256,4096]{2,1,0:T(8,128)(2,1)}, u32[]{:S(2)}) copy-start(bf16[1,256,4096]{2,1,0:T(8,128)(2,1)} %param.13) | copy-start | bytes 6291460
  6.6 361.1 %reduce-scatter.2.cloned.1.call-start = ((), (), s32[]{:S(2)}) async-start(), calls=%async_computation.5 | async-start | bytes 9437184 | tf_op jit(solution)/shard_map/reduce_scatter | solution.py:61
  75.0 188.6 %copy-start.2 = (bf16[1,4096,256]{2,1,0:T(8,128)(2,1)S(1)}, bf16[1,4096,256]{2,1,0:T(8,128)(2,1)}, u32[]{:S(2)}) copy-start(bf16[1,4096,256]{2,1,0:T(8,128)(2,1)} %param.11) | copy-start | bytes 6291460
  263.6 2.4 copy-start.6
  380.6 9.3 %copy-start.3 = (f32[256,2]{0,1:T(2,128)S(1)}, f32[256,2]{0,1:T(2,128)}, u32[]{:S(2)}) copy-start(f32[256,2]{0,1:T(2,128)} %param.10) | copy-start | bytes 6148
  382.2 35.7 %all-to-all-start.2 = ((bf16[16,2,16384]{2,1,0:T(2,128)(2,1)}), bf16[16,2,16384]{2,1,0:T(2,128)(2,1)S(1)}, u32[]{:S(2)}, u32[]{:S(2)}) async-start(bf16[16,2,16384]{2,1,0:T(2,128)(2,1)} %reshape.167), calls=%async_computation.3 | async-start | bytes 2097152 | tf_op jit(solution)/shard_map/all_to_all | solution.py:64
  425.9 5.5 %copy-start.1 = (bf16[512,512]{1,0:T(8,128)(2,1)S(1)}, bf16[512,512]{1,0:T(8,128)(2,1)}, u32[]{:S(2)}) copy-start(bf16[512,512]{1,0:T(8,128)(2,1)} %gather_fusion.1) | copy-start | bytes 1572868
  425.9 16.8 %copy-start.4 = (f32[512]{0:T(512)S(1)}, f32[512]{0:T(512)}, u32[]{:S(2)}) copy-start(f32[512]{0:T(512)} %param.15) | copy-start | bytes 6148
  425.9 16.8 %copy-start.5 = (f32[512]{0:T(512)S(1)}, f32[512]{0:T(512)}, u32[]{:S(2)}) copy-start(f32[512]{0:T(512)} %param.14) | copy-start | bytes 6148
Sparse Core Ops, SparseCore 0:
  274.2 93.3 reduce-scatter.1
